TPU v7x, 32 devices: a whole 2x2x4 slice. The times are simulated.
32 devices in a mesh: ep: 8 (over z, y), tp: 4 (over x, core).
Axes of the slice: x: 2, y: 2, z: 4, core: 2. Of those that a mesh axis runs over, the one named last changes fastest.
Arguments:
- tokens: bfloat16 [256, 2048], P('ep'), may hold values from -6 to 6
- in_gain: float32 [2048], replicated, may hold values from 0.1 to 1.9
- expert_ids: int32 [256, 2], P('ep'), may hold values from 0 to 7, all different within a row; in each aligned block of 32 rows (0 to 31, 32 to 63, ...) at most 16 rows name the same one
- route_weight: float32 [256, 2], P('ep'), may hold values from 0.1 to 1
- w_gate: bfloat16 [8, 2048, 1024], P('ep', None, 'tp'), may hold values from -0.125 to 0.125
- w_up: bfloat16 [8, 2048, 1024], P('ep', None, 'tp'), may hold values from -0.125 to 0.125
- w_down: bfloat16 [8, 1024, 2048], P('ep', 'tp'), may hold values from -0.1875 to 0.1875
- out_gain: float32 [2048], P('tp'), may hold values from 0.1 to 1.9
Outputs:
- mixed: bfloat16 [256, 2048], P('ep', 'tp')
Inputs may be any that keep to these rules, and one draw needn't show every extreme that they name: `expert_ids`: each token names 2 different experts; among the tokens of one index of ep no expert is named more than 16 times, and in every draw the tokens of some index of ep name some expert exactly 16 times; every expert is named by some token.
All inputs are finite; a program needn't handle non-finite values.
Results may differ from a plain program's by a relative error of at most 0.002.
Values may be sent and summed in bfloat16 or wider, within the bound.
A program may use at most 64 MiB of HBM per device.

v0:
```python
import jax
import jax.numpy as jnp
from jax import lax
from jax.sharding import PartitionSpec as P

norm_eps = 1e-05


def shards(tokens, in_gain, expert_ids, route_weight, w_gate, w_up, w_down, out_gain):
    tok_rows = tokens.shape[0]
    top_count = expert_ids.shape[1]
    local_experts = w_gate.shape[0]
    groups = lax.axis_size("ep")
    experts = local_experts * groups
    capacity = max(
        2, min(tok_rows // (2 * local_experts), (5 * tok_rows * top_count + experts - 1) // experts)
    )
    values = tokens.astype(jnp.float32)
    row_centre = jnp.mean(values, axis=1, keepdims=True)
    centered_in = values - row_centre
    spread_in = jnp.mean(centered_in * centered_in, axis=1, keepdims=True)
    normed = (centered_in * lax.rsqrt(spread_in + norm_eps) * in_gain).astype(jnp.bfloat16)
    routes_flat = expert_ids.reshape(-1)
    labels = lax.broadcasted_iota(jnp.int32, (1, experts), 1)
    one_hot = (routes_flat[:, None] == labels).astype(jnp.int32)
    before = jnp.cumsum(one_hot, axis=0) - one_hot
    slot_index = jnp.sum(before * one_hot, axis=1)
    positions = routes_flat * capacity + slot_index
    source = jnp.repeat(normed, top_count, axis=0)
    outgoing = (
        jnp.zeros((experts * capacity, normed.shape[1]), jnp.bfloat16).at[positions].set(source)
    )
    arrived = lax.all_to_all(outgoing, "ep", split_axis=0, concat_axis=0, tiled=True)
    arrived = arrived.reshape(groups, local_experts, capacity, normed.shape[1])
    gate_act = jnp.einsum("sjcd,jdf->sjcf", arrived, w_gate, preferred_element_type=jnp.float32)
    up_act = jnp.einsum("sjcd,jdf->sjcf", arrived, w_up, preferred_element_type=jnp.float32)
    hidden = (jax.nn.silu(gate_act) * up_act).astype(jnp.bfloat16)
    partial_value = jnp.einsum("sjcf,jfd->sjcd", hidden, w_down, preferred_element_type=jnp.float32)
    partial_value = partial_value.reshape(experts * capacity, normed.shape[1])
    weights = route_weight.reshape(-1, 1)

    def combine(returned):
        picked = returned[positions] * weights
        return jnp.sum(picked.reshape(tok_rows, top_count, -1), axis=1)

    summed = lax.psum_scatter(partial_value, "tp", scatter_dimension=1, tiled=True)
    returned = lax.all_to_all(summed, "ep", split_axis=0, concat_axis=0, tiled=True)
    mixture = combine(returned)
    full_width = mixture.shape[1] * lax.axis_size("tp")
    row_total = lax.psum(jnp.sum(mixture, axis=1, keepdims=True), "tp")
    row_mean = row_total / full_width
    centered = mixture - row_mean
    deviations = lax.psum(jnp.sum(centered * centered, axis=1, keepdims=True), "tp")
    spread = deviations / full_width
    return (centered * lax.rsqrt(spread + norm_eps) * out_gain).astype(jnp.bfloat16)


def solution(mesh):
    in_specs = (
        P("ep", None),
        P(),
        P("ep", None),
        P("ep", None),
        P("ep", None, "tp"),
        P("ep", None, "tp"),
        P("ep", "tp", None),
        P("tp"),
    )
    out_specs = P("ep", "tp")
    return jax.shard_map(shards, mesh=mesh, in_specs=in_specs, out_specs=out_specs, check_vma=False)
```

profile of v0, /device:TPU:0, one launch (start us, length us, event | category | flops | bytes accessed | tf_op | source)
XLA Modules:
  0.0 95.1 jit_solution(13158533392415035308)
XLA Ops:
  6.5 0.9 copy.14
  7.4 0.1 eq.15
  7.5 0.1 fusion.22
  7.6 0.1 reduce_window_sum.11
  7.7 0.2 select_reduce_fusion
  7.9 0.1 copy.13
  8.0 0.1 mul.84
  8.1 0.1 convert_reduce_fusion
  8.2 0.2 fusion.11
  8.4 0.5 copy-done.3
  8.9 0.1 fusion.13
  9.0 0.1 broadcast_in_dim.9
  9.2 0.1 reshape.106
  9.3 1.2 %scatter_custom_fusion = bf16[128,2048]{1,0:T(8,128)(2,1)S(1)} fusion(s32[64]{0:T(128)S(1)} %fusion.23, bf16[64,2048]{1,0:T(8,128)(2,1)S(1)} %reshape.106, bf16[]{:T(256)} %constant.8.clone.1), kind=kCustom, calls=%fused_computation.18 | custom fusion | bytes 524290 | tf_op jit(solution)/shard_map/scatter | solution.py:31
  10.5 21.8 %all_to_all.21 = bf16[8,16,2048]{2,1,0:T(8,128)(2,1)S(1)} all-to-all(bf16[8,16,2048]{2,1,0:T(8,128)(2,1)S(1)} %bitcast.64), channel_id=1, replica_groups=mesh['ep'=8,'tp'=4] {'ep'}, dimensions={0} | all-to-all | bytes 1048576 | tf_op jit(solution)/shard_map/all_to_all | solution.py:33
  32.3 0.3 convolution_bitcast_fusion.1
  32.6 3.0 %fusion.3 = f32[8,16,2048]{2,1,0:T(8,128)} fusion(bf16[1,256,2048]{2,1,0:T(8,128)(2,1)S(1)} %copy-done, bf16[8,16,2048]{2,1,0:T(8,128)(2,1)S(1)} %all_to_all.21, bf16[1,2048,256]{2,1,0:T(8,128)(2,1)} %param.13, f32[8,1,16,256]{3,2,0,1:T(8,128)S(1)} %convolution_bitcast_fusion.1), kind=kOutput, calls=%fused_computation.7 | convolution fusion | flops 268632064 | bytes 3801088 | tf_op jit(solution)/shard_map/sjcf,jfd->sjcd/dot_general | solution.py:38
  35.6 23.8 %reduce-scatter.2.cloned.1.call-done = f32[128,512]{1,0:T(8,128)} async-done(((f32[128,2048]{1,0:T(8,128)}), f32[128,512]{1,0:T(8,128)}) %reduce-scatter.2.cloned.1.call-update) | async-done | bytes 262160 | tf_op jit(solution)/shard_map/reduce_scatter | solution.py:46
  59.4 5.7 %all-to-all-start.1 = ((f32[8,16,512]{2,1,0:T(8,128)}), f32[8,16,512]{2,1,0:T(8,128)S(1)}, u32[]{:S(2)}, u32[]{:S(2)}) async-start(f32[8,16,512]{2,1,0:T(8,128)} %bitcast.65), calls=%async_computation.2 | async-start | bytes 524288 | tf_op jit(solution)/shard_map/all_to_all | solution.py:47
  65.1 0.1 copy.15
  65.2 0.1 mul.95
  65.3 9.0 %all-to-all-done.1 = f32[8,16,512]{2,1,0:T(8,128)S(1)} async-done(((f32[8,16,512]{2,1,0:T(8,128)}), f32[8,16,512]{2,1,0:T(8,128)S(1)}, u32[]{:S(2)}, u32[]{:S(2)}) %all-to-all-start.1) | async-done | bytes 262176 | tf_op jit(solution)/shard_map/all_to_all | solution.py:47
  74.3 0.7 gather_fusion
  74.9 0.1 gather.6
  75.0 0.2 multiply_reduce_fusion.1
  75.2 0.2 multiply_reduce_fusion
  75.4 0.1 reduce_sum.69
  75.5 0.1 reduce_sum.70
  75.6 6.0 %psum.14 = f32[32,1]{0,1:T(1,128)S(1)} all-reduce(f32[32,1]{0,1:T(1,128)S(1)} %bitcast.67), channel_id=1, replica_groups=mesh['ep'=8,'tp'=4] {'tp'}, use_global_device_ids=true, to_apply=%region_9.10 | all-reduce | flops 32 | bytes 256 | tf_op jit(solution)/shard_map/psum | solution.py:50
  81.6 0.2 multiply_reduce_fusion.2
  81.8 5.8 %psum.15 = f32[32,1]{0,1:T(1,128)S(1)} all-reduce(f32[32,1]{0,1:T(1,128)S(1)} %bitcast.66), channel_id=1, replica_groups=mesh['ep'=8,'tp'=4] {'tp'}, use_global_device_ids=true, to_apply=%region_11.12 | all-reduce | flops 32 | bytes 256 | tf_op jit(solution)/shard_map/psum | solution.py:53
  87.6 0.7 multiply_convert_fusion
  (22 shorter events, 0.1 us)
Async XLA Ops:
  6.5 26.1 %copy-start = (bf16[1,256,2048]{2,1,0:T(8,128)(2,1)S(1)}, bf16[1,256,2048]{2,1,0:T(8,128)(2,1)}, u32[]{:S(2)}) copy-start(bf16[1,256,2048]{2,1,0:T(8,128)(2,1)} %param.14) | copy-start | bytes 3145732
  6.5 0.9 copy-start.4
  6.5 1.5 %copy-start.1 = (bf16[32,2048]{1,0:T(8,128)(2,1)S(1)}, bf16[32,2048]{1,0:T(8,128)(2,1)}, u32[]{:S(2)}) copy-start(bf16[32,2048]{1,0:T(8,128)(2,1)} %param.8) | copy-start | bytes 393220
  6.5 52.9 %reduce-scatter.2.cloned.1.call-start = ((), (), s32[]{:S(2)}) async-start(), calls=%async_computation.3 | async-start | bytes 1310720 | tf_op jit(solution)/shard_map/reduce_scatter | solution.py:46
  8.2 0.7 copy-start.3
  9.2 23.1 %copy-start.2 = (bf16[1,2048,256]{2,1,0:T(8,128)(2,1)S(1)}, bf16[1,2048,256]{2,1,0:T(8,128)(2,1)}, u32[]{:S(2)}) copy-start(bf16[1,2048,256]{2,1,0:T(8,128)(2,1)} %param.12) | copy-start | bytes 3145732
  59.4 5.7 %copy-start.6 = (f32[32,2]{0,1:T(2,128)S(1)}, f32[32,2]{0,1:T(2,128)}, u32[]{:S(2)}) copy-start(f32[32,2]{0,1:T(2,128)} %param.11) | copy-start | bytes 772
  59.4 14.8 %all-to-all-start.1 = ((f32[8,16,512]{2,1,0:T(8,128)}), f32[8,16,512]{2,1,0:T(8,128)S(1)}, u32[]{:S(2)}, u32[]{:S(2)}) async-start(f32[8,16,512]{2,1,0:T(8,128)} %bitcast.65), calls=%async_computation.2 | async-start | bytes 524288 | tf_op jit(solution)/shard_map/all_to_all | solution.py:47
  81.8 5.8 %copy-start.5 = (f32[512]{0:T(512)S(1)}, f32[512]{0:T(512)}, u32[]{:S(2)}) copy-start(f32[512]{0:T(512)} %param.15) | copy-start | bytes 6148
Sparse Core Ops, SparseCore 0:
  35.8 23.6 reduce-scatter.1
where the time goes:
time: 95.5 us; the launch traced here: 95.1 us
  blocking collectives  33.5 us (35%)
  waiting for transfers between devices  32.8 us (34%)
  between operations  13.5 us (14%)
  starting transfers between devices  5.66 us (6%)
  local copies, waits for them, and re-layouts  4.08 us (4%)
  matrix products  3.3 us (3%)
  other arithmetic  2.24 us (2%)
    reduce_scatter x1, waiting for transfers between devices, shards(): lax.psum_scatter(partial_value, 'tp', scatter_dimension=1, tiled=True)  23.8 us
    all_to_all x1, blocking collectives, shards(): lax.all_to_all(outgoing, 'ep', split_axis=0, concat_axis=0, tiled=True)  21.8 us
    all_to_all x1, waiting for transfers between devices, shards(): lax.all_to_all(summed, 'ep', split_axis=0, concat_axis=0, tiled=True)  8.95 us
    psum x1, blocking collectives, shards(): row_total = lax.psum(jnp.sum(mixture, axis=1, keepdims=True), 'tp')  5.99 us
    psum x1, blocking collectives, shards(): lax.psum(jnp.sum(centered * centered, axis=1, keepdims=True), 'tp')  5.76 us
    all_to_all x1, starting transfers between devices, shards(): lax.all_to_all(summed, 'ep', split_axis=0, concat_axis=0, tiled=True)  5.66 us
    dot_general x1, matrix products, shards(): jnp.einsum('sjcf,jfd->sjcd', hidden, w_down, preferred_element_type=jnp.f...  3 us
  transfers between devices with their start and end apart: 2, of which 2 were waited for; matrix products, arithmetic and copies ran while one was open for 0% of the time, Pallas kernels for 0%

commit v1 on v0

--- a/solution.py
+++ b/solution.py
@@ -1,20 +1,258 @@
+import functools
+
 import jax
 import jax.numpy as jnp
 from jax import lax
+from jax.experimental import pallas as pl
+from jax.experimental.pallas import tpu as pltpu
 from jax.sharding import PartitionSpec as P
 
 norm_eps = 1e-05
-
-
-def shards(tokens, in_gain, expert_ids, route_weight, w_gate, w_up, w_down, out_gain):
+MESH = pl.DeviceIdType.MESH
+
+
+def capacity_of(tok_rows, top_count, local_experts, experts):
+    return max(
+        2, min(tok_rows // (2 * local_experts), (5 * tok_rows * top_count + experts - 1) // experts)
+    )
+
+
+def fused(
+    groups, parts, inner, cap,
+    tokens, in_gain, ids, weights, w_gate, w_up, w_down, out_gain,
+    out,
+    gate_v, up_v, down_v, sent, arrived, part, half_in, half, quarter_in, reduced, returned, stats,
+    w_sem, ep_send, ep_recv, tp_send, tp_recv, in_send, in_recv, out_send, out_recv,
+    ret_send, ret_recv, st_send, st_recv,
+):
+    outer = parts // inner
+    ep, tp = lax.axis_index("ep"), lax.axis_index("tp")
+    o, i = tp // inner, tp % inner
+    tok, width = tokens.shape
+    slots = groups * cap
+    piece = width // parts
+
+    def rows(g):
+        return pl.ds(pl.multiple_of(g * cap, cap), cap)
+
+    def cols(b):
+        return pl.ds(pl.multiple_of(b * piece, piece), piece)
+
+    barrier = pltpu.get_barrier_semaphore()
+    for off in range(1, groups):
+        pl.semaphore_signal(barrier, inc=1, device_id=((ep + off) % groups, tp), device_id_type=MESH)
+    for j in range(1, parts):
+        pl.semaphore_signal(barrier, inc=1, device_id=(ep, (tp + j) % parts), device_id_type=MESH)
+
+    loads = [
+        pltpu.make_async_copy(src.at[0], dst, w_sem.at[n])
+        for n, (src, dst) in enumerate(((w_gate, gate_v), (w_up, up_v), (w_down, down_v)))
+    ]
+    for load in loads:
+        load.start()
+
+    values = tokens[...].astype(jnp.float32)
+    centred = values - jnp.mean(values, axis=1, keepdims=True)
+    spread = jnp.mean(centred * centred, axis=1, keepdims=True)
+    normed = (centred * lax.rsqrt(spread + norm_eps) * in_gain[...]).astype(jnp.bfloat16)
+
+    lane = lax.broadcasted_iota(jnp.int32, (tok, slots), 1)
+    owner = jnp.zeros((tok, slots), jnp.int32)
+    for g in range(1, groups):
+        owner = owner + jnp.where(lane >= g * cap, 1, 0)
+    slot = (lane - owner * cap).astype(jnp.float32)
+    named = jnp.zeros((tok, slots), jnp.float32)
+    scale = jnp.zeros((tok, slots), jnp.float32)
+    for k in range(ids.shape[1]):
+        hit = ids[:, k:k + 1] == owner
+        named = named + jnp.where(hit, 1.0, 0.0)
+        scale = scale + jnp.where(hit, weights[:, k:k + 1], 0.0)
+    earlier = (
+        lax.broadcasted_iota(jnp.int32, (tok, tok), 1) < lax.broadcasted_iota(jnp.int32, (tok, tok), 0)
+    )
+    before = jnp.dot(
+        jnp.where(earlier, 1.0, 0.0).astype(jnp.bfloat16), named.astype(jnp.bfloat16),
+        preferred_element_type=jnp.float32,
+    )
+    chosen = jnp.where(before == slot, named, 0.0)
+    scale = chosen * scale
+    picked = chosen.T.astype(jnp.bfloat16)
+    sent[...] = jnp.dot(picked, normed, preferred_element_type=jnp.float32).astype(jnp.bfloat16)
+
+    pl.semaphore_wait(barrier, groups - 1 + parts - 1)
+
+    order = sorted(range(1, groups), key=lambda off: -min(off, groups - off))
+    scatter = {}
+    for off in order:
+        to = (ep + off) % groups
+        scatter[off] = pltpu.make_async_remote_copy(
+            src_ref=sent.at[rows(to), cols(tp)], dst_ref=arrived.at[rows(ep), cols(tp)],
+            send_sem=ep_send.at[off], recv_sem=ep_recv.at[off],
+            device_id=(to, tp), device_id_type=MESH,
+        )
+        scatter[off].start()
+    arrived[rows(ep), :] = sent[rows(ep), :]
+    spread_out = []
+    for off in order[::-1]:
+        came = (ep + groups - off) % groups
+        scatter[off].wait_recv()
+        for j in range(1, parts):
+            copy = pltpu.make_async_remote_copy(
+                src_ref=arrived.at[rows(came), cols(tp)], dst_ref=arrived.at[rows(came), cols(tp)],
+                send_sem=tp_send.at[off, j], recv_sem=tp_recv.at[off, j],
+                device_id=(ep, (tp + j) % parts), device_id_type=MESH,
+            )
+            copy.start()
+            spread_out.append(copy)
+    for load in loads:
+        load.wait()
+    for copy in spread_out:
+        copy.wait_recv()
+
+    inputs = arrived[...]
+    gate_act = jnp.dot(inputs, gate_v[...], preferred_element_type=jnp.float32)
+    up_act = jnp.dot(inputs, up_v[...], preferred_element_type=jnp.float32)
+    hidden = (gate_act / (1.0 + jnp.exp(-gate_act)) * up_act).astype(jnp.bfloat16)
+
+    def down(b):
+        return jnp.dot(hidden, down_v[:, cols(b)], preferred_element_type=jnp.float32)
+
+    far = [(o + j) % outer for j in range(1, outer)]
+    places = far + [o]
+    inner_copies = []
+    for n in range(1, inner):
+        other = (i + n) % inner
+        for p, place in enumerate(places):
+            part[n - 1, p] = down(place * inner + other)
+            copy = pltpu.make_async_remote_copy(
+                src_ref=part.at[n - 1, p], dst_ref=half_in.at[n - 1, p],
+                send_sem=in_send.at[n - 1, p], recv_sem=in_recv.at[n - 1, p],
+                device_id=(ep, o * inner + other), device_id_type=MESH,
+            )
+            copy.start()
+            inner_copies.append(copy)
+    for p, place in enumerate(places):
+        half[p] = down(place * inner + i)
+
+    targets = order + [0]
+    outer_copies = {}
+    for p in range(outer - 1):
+        for n in range(1, inner):
+            inner_copies[(n - 1) * outer + p].wait_recv()
+        for off in targets:
+            at = rows((ep + off) % groups)
+            total = half[p, at]
+            for n in range(1, inner):
+                total = total + half_in[n - 1, p, at]
+            half[p, at] = total
+            copy = pltpu.make_async_remote_copy(
+                src_ref=half.at[p, at], dst_ref=quarter_in.at[p, at],
+                send_sem=out_send.at[p, off], recv_sem=out_recv.at[p, off],
+                device_id=(ep, far[p] * inner + i), device_id_type=MESH,
+            )
+            copy.start()
+            outer_copies[p, off] = copy
+    for n in range(1, inner):
+        inner_copies[(n - 1) * outer + outer - 1].wait_recv()
+    back = {}
+    for off in targets:
+        to = (ep + off) % groups
+        at = rows(to)
+        total = half[outer - 1, at]
+        for n in range(1, inner):
+            total = total + half_in[n - 1, outer - 1, at]
+        for p in range(outer - 1):
+            outer_copies[p, off].wait_recv()
+            total = total + quarter_in[p, at]
+        if off == 0:
+            returned[at] = total
+        else:
+            reduced[at] = total
+            back[off] = pltpu.make_async_remote_copy(
+                src_ref=reduced.at[at], dst_ref=returned.at[rows(ep)],
+                send_sem=ret_send.at[off], recv_sem=ret_recv.at[off],
+                device_id=(to, tp), device_id_type=MESH,
+            )
+            back[off].start()
+    for off in order:
+        back[off].wait_recv()
+
+    mixture = jnp.dot(
+        scale, returned[...], precision=lax.Precision.HIGHEST, preferred_element_type=jnp.float32
+    )
+    own_mean = jnp.mean(mixture, axis=1, keepdims=True)
+    own_gap = mixture - own_mean
+    own_spread = jnp.sum(own_gap * own_gap, axis=1, keepdims=True)
+    column = lax.broadcasted_iota(jnp.int32, (tok, 128), 1)
+    stats[0] = jnp.where(column == 0, own_mean, own_spread)
+    moments = []
+    for j in range(1, parts):
+        copy = pltpu.make_async_remote_copy(
+            src_ref=stats.at[0], dst_ref=stats.at[j],
+            send_sem=st_send.at[j], recv_sem=st_recv.at[j],
+            device_id=(ep, (tp + j) % parts), device_id_type=MESH,
+        )
+        copy.start()
+        moments.append(copy)
+    for copy in moments:
+        copy.wait_recv()
+    means = [own_mean] + [stats[j][:, 0:1] for j in range(1, parts)]
+    spreads = [own_spread] + [stats[j][:, 1:2] for j in range(1, parts)]
+    row_mean = sum(means) / parts
+    total = sum(spreads)
+    for mean in means:
+        total = total + piece * (mean - row_mean) * (mean - row_mean)
+    out[...] = (
+        (mixture - row_mean) * lax.rsqrt(total / width + norm_eps) * out_gain[...]
+    ).astype(out.dtype)
+
+    for off in order:
+        scatter[off].wait_send()
+        back[off].wait_send()
+    for copy in spread_out + inner_copies + list(outer_copies.values()) + moments:
+        copy.wait_send()
+
+
+def one_kernel(groups, parts, cap, tokens, in_gain, ids, weights, w_gate, w_up, w_down, out_gain):
+    inner = 2
+    outer = parts // inner
+    tok, width = tokens.shape
+    slots, piece, hidden = groups * cap, width // parts, w_gate.shape[2]
+    vmem, hbm, dma = pl.BlockSpec(memory_space=pltpu.VMEM), pl.BlockSpec(memory_space=pl.ANY), pltpu.SemaphoreType.DMA
+    return pl.pallas_call(
+        functools.partial(fused, groups, parts, inner, cap),
+        name="experts",
+        out_shape=jax.ShapeDtypeStruct((tok, piece), jnp.bfloat16),
+        in_specs=[vmem, vmem, vmem, vmem, hbm, hbm, hbm, vmem],
+        out_specs=vmem,
+        scratch_shapes=[
+            pltpu.VMEM((width, hidden), jnp.bfloat16),
+            pltpu.VMEM((width, hidden), jnp.bfloat16),
+            pltpu.VMEM((hidden, width), jnp.bfloat16),
+            pltpu.VMEM((slots, width), jnp.bfloat16),
+            pltpu.VMEM((slots, width), jnp.bfloat16),
+            pltpu.VMEM((inner - 1, outer, slots, piece), jnp.float32),
+            pltpu.VMEM((inner - 1, outer, slots, piece), jnp.float32),
+            pltpu.VMEM((outer, slots, piece), jnp.float32),
+            pltpu.VMEM((outer, slots, piece), jnp.float32),
+            pltpu.VMEM((slots, piece), jnp.float32),
+            pltpu.VMEM((slots, piece), jnp.float32),
+            pltpu.VMEM((parts, tok, 128), jnp.float32),
+            dma((3,)), dma((groups,)), dma((groups,)), dma((groups, parts)), dma((groups, parts)),
+            dma((inner - 1, outer)), dma((inner - 1, outer)), dma((outer, groups)), dma((outer, groups)),
+            dma((groups,)), dma((groups,)), dma((parts,)), dma((parts,)),
+        ],
+        compiler_params=pltpu.CompilerParams(collective_id=0, has_side_effects=True),
+    )(tokens, in_gain.reshape(1, -1), ids, weights, w_gate, w_up, w_down, out_gain.reshape(1, -1))
+
+
+def collectives(tokens, in_gain, expert_ids, route_weight, w_gate, w_up, w_down, out_gain):
     tok_rows = tokens.shape[0]
     top_count = expert_ids.shape[1]
     local_experts = w_gate.shape[0]
     groups = lax.axis_size("ep")
     experts = local_experts * groups
-    capacity = max(
-        2, min(tok_rows // (2 * local_experts), (5 * tok_rows * top_count + experts - 1) // experts)
-    )
+    capacity = capacity_of(tok_rows, top_count, local_experts, experts)
     values = tokens.astype(jnp.float32)
     row_centre = jnp.mean(values, axis=1, keepdims=True)
     centered_in = values - row_centre
@@ -55,6 +293,21 @@
     return (centered * lax.rsqrt(spread + norm_eps) * out_gain).astype(jnp.bfloat16)
 
 
+def shards(tokens, in_gain, expert_ids, route_weight, w_gate, w_up, w_down, out_gain):
+    groups, parts = lax.axis_size("ep"), lax.axis_size("tp")
+    tok_rows, width = tokens.shape
+    local_experts = w_gate.shape[0]
+    cap = capacity_of(tok_rows, expert_ids.shape[1], local_experts, local_experts * groups)
+    whole_tiles = cap % 16 == 0 and (groups * cap) % 128 == 0 and width % (parts * 128) == 0
+    if local_experts == 1 and parts % 2 == 0 and whole_tiles and groups * cap * width <= 1 << 20:
+        return one_kernel(
+            groups, parts, cap, tokens, in_gain, expert_ids, route_weight, w_gate, w_up, w_down, out_gain
+        )
+    return collectives(
+        tokens, in_gain, expert_ids, route_weight, w_gate, w_up, w_down, out_gain
+    )
+
+
 def solution(mesh):
     in_specs = (
         P("ep", None),

time: 95.5 us -> 39.4 us (0.41)
  Pallas kernels: 0 us -> 35.8 us
  blocking collectives: 33.5 us -> 0 us
  waiting for transfers between devices: 32.8 us -> 0 us
  between operations: 13.5 us -> 0.01 us
  starting transfers between devices: 5.66 us -> 0 us
  matrix products: 3.3 us -> 0 us
  other arithmetic: 2.24 us -> 0 us
    pallas_call x0 -> x1, Pallas kernels: none -> 35.8 us  [one_kernel(): pl.pallas_call(functools.partial(fused, groups, parts, inner, cap), name=...]
    reduce_scatter x1 -> x0, waiting for transfers between devices: 23.8 us -> none  [shards(): lax.psum_scatter(partial_value, 'tp', scatter_dimension=1, tiled=True)]
    all_to_all x1 -> x0, blocking collectives: 21.8 us -> none  [shards(): lax.all_to_all(outgoing, 'ep', split_axis=0, concat_axis=0, tiled=True)]
    psum x2 -> x0, blocking collectives: 11.7 us -> none  [the longest x1 5.99 us: shards(): row_total = lax.psum(jnp.sum(mixture, axis=1, keepdims=True), 'tp')]
    all_to_all x1 -> x0, waiting for transfers between devices: 8.95 us -> none  [shards(): lax.all_to_all(summed, 'ep', split_axis=0, concat_axis=0, tiled=True)]
    all_to_all x1 -> x0, starting transfers between devices: 5.66 us -> none  [shards(): lax.all_to_all(summed, 'ep', split_axis=0, concat_axis=0, tiled=True)]
    dot_general x2 -> x0, matrix products: 3.3 us -> none  [the longest x1 3 us: shards(): jnp.einsum('sjcf,jfd->sjcd', hidden, w_down, preferred_element_type=jnp.f...]
    unnamed x16 -> x7, local copies, waits for them, and re-layouts: 1.44 us -> 3.43 us
  transfers between devices with their start and end apart: 2 -> 0, of which waited for: 2 -> 0; matrix products, arithmetic and copies ran while one was open for 0% -> 0% of each run, Pallas kernels for 0% -> 0%
where the time goes in v1:
time: 39.4 us; the launch traced here: 39.2 us
  Pallas kernels  35.8 us (91%)
  local copies, waits for them, and re-layouts  3.43 us (9%)
    pallas_call x1, Pallas kernels, one_kernel(): pl.pallas_call(functools.partial(fused, groups, parts, inner, cap), name=...  35.8 us
    unnamed x7, local copies, waits for them, and re-layouts  3.43 us

profile of v1, /device:TPU:0, one launch (start us, length us, event | category | flops | bytes accessed | tf_op | source)
XLA Modules:
  0.0 39.2 jit_solution(9143870880700155709)
XLA Ops:
  0.0 0.0 copy-start
  0.0 0.7 %copy-done = s32[32,2]{0,1:T(2,128)S(1)} copy-done((s32[32,2]{0,1:T(2,128)S(1)}, s32[32,2]{0,1:T(2,128)}, u32[]{:S(2)}) %copy-start) | copy-done | bytes 280
  0.7 0.0 copy-start.1
  0.7 0.7 %copy.9.ids = s32[32,2]{1,0:T(8,128)} copy(s32[32,2]{0,1:T(2,128)S(1)} %copy-done) | data formatting | bytes 512 | tf_op args[2]
  1.4 0.0 copy-done.1
  1.4 0.7 %copy.10.weights = f32[32,2]{1,0:T(8,128)} copy(f32[32,2]{0,1:T(2,128)S(1)} %copy-done.1) | data formatting | bytes 512 | tf_op args[3]
  2.1 35.8 %experts.1 = bf16[32,512]{1,0:T(8,128)(2,1)} custom-call(bf16[32,2048]{1,0:T(8,128)(2,1)} %tokens.1, f32[1,2048]{1,0:T(1,128)} %bitcast.2, s32[32,2]{1,0:T(8,128)} %copy.9.ids, f32[32,2]{1,0:T(8,128)} %copy.10.weights, bf16[1,2048,256]{2,1,0:T(8,128)(2,1)} %w_gate.1, bf16[1,2048,256]{2,1,0:T(8,128)(2,1)} %w_up.1, bf16[1,256,2048]{2,1,0:T(8,128)(2,1)} %w_down.1, ...), custom_call_target="tpu_custom_call" | custom-call | tf_op jit(solution)/shard_map/experts/pallas_call | solution.py:222
  37.8 1.4 %copy.12 = bf16[32,512]{1,0:T(8,128)(2,1)} copy(bf16[32,512]{1,0:T(8,128)(2,1)} %experts.1) | data formatting | bytes 65536
Async XLA Ops:
  0.0 0.7 %copy-start = (s32[32,2]{0,1:T(2,128)S(1)}, s32[32,2]{0,1:T(2,128)}, u32[]{:S(2)}) copy-start(s32[32,2]{0,1:T(2,128)} %param.10) | copy-start | bytes 772
  0.7 0.7 %copy-start.1 = (f32[32,2]{0,1:T(2,128)S(1)}, f32[32,2]{0,1:T(2,128)}, u32[]{:S(2)}) copy-start(f32[32,2]{0,1:T(2,128)} %param.11) | copy-start | bytes 772

commit v2 on v1

--- a/solution.py
+++ b/solution.py
@@ -19,8 +19,9 @@
 
 def fused(
     groups, parts, inner, cap,
-    tokens, in_gain, ids, weights, w_gate, w_up, w_down, out_gain,
-    out,
+    tokens_h, in_gain_h, ids_h, weights_h, w_gate, w_up, w_down, out_gain_h,
+    out_h,
+    tokens, in_gain, ids, weights, out_gain, out, picked, row_sem,
     gate_v, up_v, down_v, sent, arrived, part, half_in, half, quarter_in, reduced, returned, stats,
     w_sem, ep_send, ep_recv, tp_send, tp_recv, in_send, in_recv, out_send, out_recv,
     ret_send, ret_recv, st_send, st_recv,
@@ -44,6 +45,15 @@
     for j in range(1, parts):
         pl.semaphore_signal(barrier, inc=1, device_id=(ep, (tp + j) % parts), device_id_type=MESH)
 
+    row_loads = [
+        pltpu.make_async_copy(src, dst, row_sem.at[n])
+        for n, (src, dst) in enumerate((
+            (tokens_h, tokens), (in_gain_h, in_gain), (ids_h, ids), (weights_h, weights),
+            (out_gain_h, out_gain),
+        ))
+    ]
+    for load in row_loads:
+        load.start()
     loads = [
         pltpu.make_async_copy(src.at[0], dst, w_sem.at[n])
         for n, (src, dst) in enumerate(((w_gate, gate_v), (w_up, up_v), (w_down, down_v)))
@@ -51,33 +61,36 @@
     for load in loads:
         load.start()
 
+    for load in row_loads:
+        load.wait()
     values = tokens[...].astype(jnp.float32)
     centred = values - jnp.mean(values, axis=1, keepdims=True)
     spread = jnp.mean(centred * centred, axis=1, keepdims=True)
     normed = (centred * lax.rsqrt(spread + norm_eps) * in_gain[...]).astype(jnp.bfloat16)
 
-    lane = lax.broadcasted_iota(jnp.int32, (tok, slots), 1)
-    owner = jnp.zeros((tok, slots), jnp.int32)
+    lane = lax.broadcasted_iota(jnp.int32, (slots, tok), 0)
+    owner = jnp.zeros((slots, tok), jnp.int32)
     for g in range(1, groups):
         owner = owner + jnp.where(lane >= g * cap, 1, 0)
     slot = (lane - owner * cap).astype(jnp.float32)
-    named = jnp.zeros((tok, slots), jnp.float32)
-    scale = jnp.zeros((tok, slots), jnp.float32)
-    for k in range(ids.shape[1]):
-        hit = ids[:, k:k + 1] == owner
+    named = jnp.zeros((slots, tok), jnp.float32)
+    scale = jnp.zeros((slots, tok), jnp.float32)
+    for k in range(ids.shape[0]):
+        hit = ids[k:k + 1, :] == owner
         named = named + jnp.where(hit, 1.0, 0.0)
-        scale = scale + jnp.where(hit, weights[:, k:k + 1], 0.0)
+        scale = scale + jnp.where(hit, weights[k:k + 1, :], 0.0)
     earlier = (
-        lax.broadcasted_iota(jnp.int32, (tok, tok), 1) < lax.broadcasted_iota(jnp.int32, (tok, tok), 0)
+        lax.broadcasted_iota(jnp.int32, (tok, tok), 0) < lax.broadcasted_iota(jnp.int32, (tok, tok), 1)
     )
     before = jnp.dot(
-        jnp.where(earlier, 1.0, 0.0).astype(jnp.bfloat16), named.astype(jnp.bfloat16),
+        named.astype(jnp.bfloat16), jnp.where(earlier, 1.0, 0.0).astype(jnp.bfloat16),
         preferred_element_type=jnp.float32,
     )
     chosen = jnp.where(before == slot, named, 0.0)
-    scale = chosen * scale
-    picked = chosen.T.astype(jnp.bfloat16)
-    sent[...] = jnp.dot(picked, normed, preferred_element_type=jnp.float32).astype(jnp.bfloat16)
+    picked[...] = chosen * scale
+    sent[...] = jnp.dot(
+        chosen.astype(jnp.bfloat16), normed, preferred_element_type=jnp.float32
+    ).astype(jnp.bfloat16)
 
     pl.semaphore_wait(barrier, groups - 1 + parts - 1)
 
@@ -92,21 +105,34 @@
         )
         scatter[off].start()
     arrived[rows(ep), :] = sent[rows(ep), :]
-    spread_out = []
+    spread_out, relays, local = [], {}, []
+
+    def share(off, block, j, to):
+        came = (ep + groups - off) % groups
+        copy = pltpu.make_async_remote_copy(
+            src_ref=arrived.at[rows(came), cols(block)], dst_ref=arrived.at[rows(came), cols(block)],
+            send_sem=tp_send.at[off, j], recv_sem=tp_recv.at[off, j],
+            device_id=(ep, to), device_id_type=MESH,
+        )
+        copy.start()
+        spread_out.append(copy)
+        return copy
+
     for off in order[::-1]:
-        came = (ep + groups - off) % groups
         scatter[off].wait_recv()
-        for j in range(1, parts):
-            copy = pltpu.make_async_remote_copy(
-                src_ref=arrived.at[rows(came), cols(tp)], dst_ref=arrived.at[rows(came), cols(tp)],
-                send_sem=tp_send.at[off, j], recv_sem=tp_recv.at[off, j],
-                device_id=(ep, (tp + j) % parts), device_id_type=MESH,
-            )
-            copy.start()
-            spread_out.append(copy)
+        for a in range(1, outer):
+            relays[off, a] = share(off, tp, a * inner, (o + a) % outer * inner + i)
+        for b in range(1, inner):
+            local.append(share(off, tp, b, o * inner + (i + b) % inner))
+    for off in order[::-1]:
+        for a in range(1, outer):
+            relays[off, a].wait_recv()
+            block = (o + outer - a) % outer * inner + i
+            for b in range(1, inner):
+                local.append(share(off, block, a * inner + b, o * inner + (i + b) % inner))
     for load in loads:
         load.wait()
-    for copy in spread_out:
+    for copy in local:
         copy.wait_recv()
 
     inputs = arrived[...]
@@ -178,7 +204,7 @@
         back[off].wait_recv()
 
     mixture = jnp.dot(
-        scale, returned[...], precision=lax.Precision.HIGHEST, preferred_element_type=jnp.float32
+        picked[...].T, returned[...], precision=lax.Precision.HIGHEST, preferred_element_type=jnp.float32
     )
     own_mean = jnp.mean(mixture, axis=1, keepdims=True)
     own_gap = mixture - own_mean
@@ -205,12 +231,15 @@
     out[...] = (
         (mixture - row_mean) * lax.rsqrt(total / width + norm_eps) * out_gain[...]
     ).astype(out.dtype)
+    result = pltpu.make_async_copy(out, out_h, row_sem.at[0])
+    result.start()
 
     for off in order:
         scatter[off].wait_send()
         back[off].wait_send()
     for copy in spread_out + inner_copies + list(outer_copies.values()) + moments:
         copy.wait_send()
+    result.wait()
 
 
 def one_kernel(groups, parts, cap, tokens, in_gain, ids, weights, w_gate, w_up, w_down, out_gain):
@@ -218,14 +247,22 @@
     outer = parts // inner
     tok, width = tokens.shape
     slots, piece, hidden = groups * cap, width // parts, w_gate.shape[2]
-    vmem, hbm, dma = pl.BlockSpec(memory_space=pltpu.VMEM), pl.BlockSpec(memory_space=pl.ANY), pltpu.SemaphoreType.DMA
+    hbm, dma = pl.BlockSpec(memory_space=pl.ANY), pltpu.SemaphoreType.DMA
     return pl.pallas_call(
         functools.partial(fused, groups, parts, inner, cap),
         name="experts",
         out_shape=jax.ShapeDtypeStruct((tok, piece), jnp.bfloat16),
-        in_specs=[vmem, vmem, vmem, vmem, hbm, hbm, hbm, vmem],
-        out_specs=vmem,
+        in_specs=[hbm] * 8,
+        out_specs=hbm,
         scratch_shapes=[
+            pltpu.VMEM((tok, width), jnp.bfloat16),
+            pltpu.VMEM((1, width), jnp.float32),
+            pltpu.VMEM(ids.shape, jnp.int32),
+            pltpu.VMEM(ids.shape, jnp.float32),
+            pltpu.VMEM((1, piece), jnp.float32),
+            pltpu.VMEM((tok, piece), jnp.bfloat16),
+            pltpu.VMEM((slots, tok), jnp.float32),
+            dma((5,)),
             pltpu.VMEM((width, hidden), jnp.bfloat16),
             pltpu.VMEM((width, hidden), jnp.bfloat16),
             pltpu.VMEM((hidden, width), jnp.bfloat16),
@@ -301,7 +338,7 @@
     whole_tiles = cap % 16 == 0 and (groups * cap) % 128 == 0 and width % (parts * 128) == 0
     if local_experts == 1 and parts % 2 == 0 and whole_tiles and groups * cap * width <= 1 << 20:
         return one_kernel(
-            groups, parts, cap, tokens, in_gain, expert_ids, route_weight, w_gate, w_up, w_down, out_gain
+            groups, parts, cap, tokens, in_gain, expert_ids.T, route_weight.T, w_gate, w_up, w_down, out_gain
         )
     return collectives(
         tokens, in_gain, expert_ids, route_weight, w_gate, w_up, w_down, out_gain

time: 39.4 us -> 35.3 us (0.90)
  local copies, waits for them, and re-layouts: 3.43 us -> 1.38 us
  Pallas kernels: 35.8 us -> 33.8 us
    unnamed x7 -> x1, local copies, waits for them, and re-layouts: 3.43 us -> 1.38 us
    pallas_call x1, Pallas kernels: 35.8 us -> 33.8 us  [one_kernel(): pl.pallas_call(functools.partial(fused, groups, parts, inner, cap), name=...]
where the time goes in v2:
time: 35.3 us; the launch traced here: 35.2 us
  Pallas kernels  33.8 us (96%)
  local copies, waits for them, and re-layouts  1.38 us (4%)
    pallas_call x1, Pallas kernels, one_kernel(): pl.pallas_call(functools.partial(fused, groups, parts, inner, cap), name=...  33.8 us
    unnamed x1, local copies, waits for them, and re-layouts  1.38 us

profile of v2, /device:TPU:0, one launch (start us, length us, event | category | flops | bytes accessed | tf_op | source)
XLA Modules:
  0.0 35.2 jit_solution(16431277845881076827)
XLA Ops:
  0.0 33.8 %experts.1 = bf16[32,512]{1,0:T(8,128)(2,1)} custom-call(bf16[32,2048]{1,0:T(8,128)(2,1)} %tokens_h.1, f32[1,2048]{1,0:T(1,128)} %bitcast.4, s32[2,32]{1,0:T(2,128)} %bitcast.6, f32[2,32]{1,0:T(2,128)} %bitcast.7, bf16[1,2048,256]{2,1,0:T(8,128)(2,1)} %w_gate.1, bf16[1,2048,256]{2,1,0:T(8,128)(2,1)} %w_up.1, bf16[1,256,2048]{2,1,0:T(8,128)(2,1)} %w_down.1, ...), custom_call_target="tpu_custom_call" | custom-call | tf_op jit(solution)/shard_map/experts/pallas_call | solution.py:251
  33.8 1.4 %copy.10 = bf16[32,512]{1,0:T(8,128)(2,1)} copy(bf16[32,512]{1,0:T(8,128)(2,1)} %experts.1) | data formatting | bytes 65536

commit v3 on v2

--- a/solution.py
+++ b/solution.py
@@ -118,13 +118,13 @@
         spread_out.append(copy)
         return copy
 
-    for off in order[::-1]:
+    for off in order:
         scatter[off].wait_recv()
         for a in range(1, outer):
             relays[off, a] = share(off, tp, a * inner, (o + a) % outer * inner + i)
         for b in range(1, inner):
             local.append(share(off, tp, b, o * inner + (i + b) % inner))
-    for off in order[::-1]:
+    for off in order:
         for a in range(1, outer):
             relays[off, a].wait_recv()
             block = (o + outer - a) % outer * inner + i

time: 35.3 us -> 34.3 us (0.972)
  Pallas kernels: 33.8 us -> 32.7 us
    pallas_call x1, Pallas kernels: 33.8 us -> 32.7 us  [one_kernel(): pl.pallas_call(functools.partial(fused, groups, parts, inner, cap), name=...]
where the time goes in v3:
time: 34.3 us; the launch traced here: 34.1 us
  Pallas kernels  32.7 us (95%)
  local copies, waits for them, and re-layouts  1.38 us (4%)
    pallas_call x1, Pallas kernels, one_kernel(): pl.pallas_call(functools.partial(fused, groups, parts, inner, cap), name=...  32.7 us
    unnamed x1, local copies, waits for them, and re-layouts  1.38 us

profile of v3, /device:TPU:0, one launch (start us, length us, event | category | flops | bytes accessed | tf_op | source)
XLA Modules:
  0.0 34.1 jit_solution(8372034586392029538)
XLA Ops:
  0.0 32.7 %experts.1 = bf16[32,512]{1,0:T(8,128)(2,1)} custom-call(bf16[32,2048]{1,0:T(8,128)(2,1)} %tokens_h.1, f32[1,2048]{1,0:T(1,128)} %bitcast.4, s32[2,32]{1,0:T(2,128)} %bitcast.6, f32[2,32]{1,0:T(2,128)} %bitcast.7, bf16[1,2048,256]{2,1,0:T(8,128)(2,1)} %w_gate.1, bf16[1,2048,256]{2,1,0:T(8,128)(2,1)} %w_up.1, bf16[1,256,2048]{2,1,0:T(8,128)(2,1)} %w_down.1, ...), custom_call_target="tpu_custom_call" | custom-call | tf_op jit(solution)/shard_map/experts/pallas_call | solution.py:251
  32.7 1.4 %copy.10 = bf16[32,512]{1,0:T(8,128)(2,1)} copy(bf16[32,512]{1,0:T(8,128)(2,1)} %experts.1) | data formatting | bytes 65536

commit v4 on v3

--- a/solution.py
+++ b/solution.py
@@ -17,12 +17,25 @@
     )
 
 
+def encode(values):
+    peak = jnp.maximum(jnp.max(jnp.abs(values), axis=1, keepdims=True), 2.0 ** -100)
+    power = jnp.floor(jnp.log2(peak)) - 14.0
+    whole = jnp.clip(jnp.round(values * jnp.exp2(-power)), -32767.0, 32767.0)
+    power = jnp.broadcast_to(power, (values.shape[0], 128))
+    return jnp.concatenate([whole, power], axis=1).astype(jnp.int32).astype(jnp.int16)
+
+
+def decode(code):
+    code = code.astype(jnp.int32).astype(jnp.float32)
+    return code[:, :-128] * jnp.exp2(code[:, -128:-127])
+
+
 def fused(
     groups, parts, inner, cap,
     tokens_h, in_gain_h, ids_h, weights_h, w_gate, w_up, w_down, out_gain_h,
     out_h,
     tokens, in_gain, ids, weights, out_gain, out, picked, row_sem,
-    gate_v, up_v, down_v, sent, arrived, part, half_in, half, quarter_in, reduced, returned, stats,
+    gate_v, up_v, down_v, sent, arrived, part, half_in, half, quarter, quarter_in, reduced, returned, stats,
     w_sem, ep_send, ep_recv, tp_send, tp_recv, in_send, in_recv, out_send, out_recv,
     ret_send, ret_recv, st_send, st_recv,
 ):
@@ -170,9 +183,9 @@
             total = half[p, at]
             for n in range(1, inner):
                 total = total + half_in[n - 1, p, at]
-            half[p, at] = total
+            quarter[p, at] = encode(total)
             copy = pltpu.make_async_remote_copy(
-                src_ref=half.at[p, at], dst_ref=quarter_in.at[p, at],
+                src_ref=quarter.at[p, at], dst_ref=quarter_in.at[p, at],
                 send_sem=out_send.at[p, off], recv_sem=out_recv.at[p, off],
                 device_id=(ep, far[p] * inner + i), device_id_type=MESH,
             )
@@ -189,11 +202,11 @@
             total = total + half_in[n - 1, outer - 1, at]
         for p in range(outer - 1):
             outer_copies[p, off].wait_recv()
-            total = total + quarter_in[p, at]
+            total = total + decode(quarter_in[p, at])
         if off == 0:
-            returned[at] = total
+            returned[at] = encode(total)
         else:
-            reduced[at] = total
+            reduced[at] = encode(total)
             back[off] = pltpu.make_async_remote_copy(
                 src_ref=reduced.at[at], dst_ref=returned.at[rows(ep)],
                 send_sem=ret_send.at[off], recv_sem=ret_recv.at[off],
@@ -204,7 +217,7 @@
         back[off].wait_recv()
 
     mixture = jnp.dot(
-        picked[...].T, returned[...], precision=lax.Precision.HIGHEST, preferred_element_type=jnp.float32
+        picked[...].T, decode(returned[...]), precision=lax.Precision.HIGHEST, preferred_element_type=jnp.float32
     )
     own_mean = jnp.mean(mixture, axis=1, keepdims=True)
     own_gap = mixture - own_mean
@@ -271,9 +284,10 @@
             pltpu.VMEM((inner - 1, outer, slots, piece), jnp.float32),
             pltpu.VMEM((inner - 1, outer, slots, piece), jnp.float32),
             pltpu.VMEM((outer, slots, piece), jnp.float32),
-            pltpu.VMEM((outer, slots, piece), jnp.float32),
-            pltpu.VMEM((slots, piece), jnp.float32),
-            pltpu.VMEM((slots, piece), jnp.float32),
+            pltpu.VMEM((outer, slots, piece + 128), jnp.int16),
+            pltpu.VMEM((outer, slots, piece + 128), jnp.int16),
+            pltpu.VMEM((slots, piece + 128), jnp.int16),
+            pltpu.VMEM((slots, piece + 128), jnp.int16),
             pltpu.VMEM((parts, tok, 128), jnp.float32),
             dma((3,)), dma((groups,)), dma((groups,)), dma((groups, parts)), dma((groups, parts)),
             dma((inner - 1, outer)), dma((inner - 1, outer)), dma((outer, groups)), dma((outer, groups)),

time: 34.3 us -> 32.6 us (0.950)
  Pallas kernels: 32.7 us -> 31.1 us
    pallas_call x1, Pallas kernels: 32.7 us -> 31.1 us  [one_kernel(): pl.pallas_call(functools.partial(fused, groups, parts, inner, cap), name=...]
where the time goes in v4:
time: 32.6 us; the launch traced here: 32.5 us
  Pallas kernels  31.1 us (95%)
  local copies, waits for them, and re-layouts  1.38 us (4%)
    pallas_call x1, Pallas kernels, one_kernel(): pl.pallas_call(functools.partial(fused, groups, parts, inner, cap), name=...  31.1 us
    unnamed x1, local copies, waits for them, and re-layouts  1.38 us

profile of v4, /device:TPU:0, one launch (start us, length us, event | category | flops | bytes accessed | tf_op | source)
XLA Modules:
  0.0 32.5 jit_solution(4283608096122119082)
XLA Ops:
  0.0 31.1 %experts.1 = bf16[32,512]{1,0:T(8,128)(2,1)} custom-call(bf16[32,2048]{1,0:T(8,128)(2,1)} %tokens_h.1, f32[1,2048]{1,0:T(1,128)} %bitcast.4, s32[2,32]{1,0:T(2,128)} %bitcast.6, f32[2,32]{1,0:T(2,128)} %bitcast.7, bf16[1,2048,256]{2,1,0:T(8,128)(2,1)} %w_gate.1, bf16[1,2048,256]{2,1,0:T(8,128)(2,1)} %w_up.1, bf16[1,256,2048]{2,1,0:T(8,128)(2,1)} %w_down.1, ...), custom_call_target="tpu_custom_call" | custom-call | tf_op jit(solution)/shard_map/experts/pallas_call | solution.py:264
  31.1 1.4 %copy.10 = bf16[32,512]{1,0:T(8,128)(2,1)} copy(bf16[32,512]{1,0:T(8,128)(2,1)} %experts.1) | data formatting | bytes 65536

commit v5 on v4

--- a/solution.py
+++ b/solution.py
@@ -158,32 +158,32 @@
 
     far = [(o + j) % outer for j in range(1, outer)]
     places = far + [o]
-    inner_copies = []
-    for n in range(1, inner):
-        other = (i + n) % inner
-        for p, place in enumerate(places):
+    halves = {}
+    for p, place in enumerate(places):
+        for n in range(1, inner):
+            other = (i + n) % inner
             part[n - 1, p] = down(place * inner + other)
-            copy = pltpu.make_async_remote_copy(
+            halves[n, p] = pltpu.make_async_remote_copy(
                 src_ref=part.at[n - 1, p], dst_ref=half_in.at[n - 1, p],
                 send_sem=in_send.at[n - 1, p], recv_sem=in_recv.at[n - 1, p],
                 device_id=(ep, o * inner + other), device_id_type=MESH,
             )
-            copy.start()
-            inner_copies.append(copy)
-    for p, place in enumerate(places):
-        half[p] = down(place * inner + i)
+            halves[n, p].start()
+        if p < outer - 1:
+            half[p] = down(place * inner + i)
+    inner_copies = list(halves.values())
 
     targets = order + [0]
     outer_copies = {}
     for p in range(outer - 1):
         for n in range(1, inner):
-            inner_copies[(n - 1) * outer + p].wait_recv()
+            halves[n, p].wait_recv()
+        total = half[p]
+        for n in range(1, inner):
+            total = total + half_in[n - 1, p]
+        quarter[p] = encode(total)
         for off in targets:
             at = rows((ep + off) % groups)
-            total = half[p, at]
-            for n in range(1, inner):
-                total = total + half_in[n - 1, p, at]
-            quarter[p, at] = encode(total)
             copy = pltpu.make_async_remote_copy(
                 src_ref=quarter.at[p, at], dst_ref=quarter_in.at[p, at],
                 send_sem=out_send.at[p, off], recv_sem=out_recv.at[p, off],
@@ -191,8 +191,9 @@
             )
             copy.start()
             outer_copies[p, off] = copy
+    half[outer - 1] = down(o * inner + i)
     for n in range(1, inner):
-        inner_copies[(n - 1) * outer + outer - 1].wait_recv()
+        halves[n, outer - 1].wait_recv()
     back = {}
     for off in targets:
         to = (ep + off) % groups
@@ -223,7 +224,7 @@
     own_gap = mixture - own_mean
     own_spread = jnp.sum(own_gap * own_gap, axis=1, keepdims=True)
     column = lax.broadcasted_iota(jnp.int32, (tok, 128), 1)
-    stats[0] = jnp.where(column == 0, own_mean, own_spread)
+    stats[0] = jnp.where(column == 0, own_mean, own_spread).T[0:8, :]
     moments = []
     for j in range(1, parts):
         copy = pltpu.make_async_remote_copy(
@@ -235,14 +236,17 @@
         moments.append(copy)
     for copy in moments:
         copy.wait_recv()
-    means = [own_mean] + [stats[j][:, 0:1] for j in range(1, parts)]
-    spreads = [own_spread] + [stats[j][:, 1:2] for j in range(1, parts)]
+    means = [stats[j][0:1, :] for j in range(parts)]
+    spreads = [stats[j][1:2, :] for j in range(parts)]
     row_mean = sum(means) / parts
     total = sum(spreads)
     for mean in means:
         total = total + piece * (mean - row_mean) * (mean - row_mean)
+    factor = lax.rsqrt(total / width + norm_eps)
+    line = lax.broadcasted_iota(jnp.int32, (8, tok), 0)
+    both = jnp.where(line == 0, row_mean, factor).T
     out[...] = (
-        (mixture - row_mean) * lax.rsqrt(total / width + norm_eps) * out_gain[...]
+        (mixture - both[:, 0:1]) * both[:, 1:2] * out_gain[...]
     ).astype(out.dtype)
     result = pltpu.make_async_copy(out, out_h, row_sem.at[0])
     result.start()
@@ -288,7 +292,7 @@
             pltpu.VMEM((outer, slots, piece + 128), jnp.int16),
             pltpu.VMEM((slots, piece + 128), jnp.int16),
             pltpu.VMEM((slots, piece + 128), jnp.int16),
-            pltpu.VMEM((parts, tok, 128), jnp.float32),
+            pltpu.VMEM((parts, 8, tok), jnp.float32),
             dma((3,)), dma((groups,)), dma((groups,)), dma((groups, parts)), dma((groups, parts)),
             dma((inner - 1, outer)), dma((inner - 1, outer)), dma((outer, groups)), dma((outer, groups)),
             dma((groups,)), dma((groups,)), dma((parts,)), dma((parts,)),

time: 32.6 us -> 32.6 us (level)
  no operation moved by 1% of the time
where the time goes in v5:
time: 32.6 us; the launch traced here: 32.4 us
  Pallas kernels  31 us (95%)
  local copies, waits for them, and re-layouts  1.38 us (4%)
    pallas_call x1, Pallas kernels, one_kernel(): pl.pallas_call(functools.partial(fused, groups, parts, inner, cap), name=...  31 us
    unnamed x1, local copies, waits for them, and re-layouts  1.38 us

profile of v5, /device:TPU:0, one launch (start us, length us, event | category | flops | bytes accessed | tf_op | source)
XLA Modules:
  0.0 32.4 jit_solution(15353197784751152933)
XLA Ops:
  0.0 31.0 %experts.1 = bf16[32,512]{1,0:T(8,128)(2,1)} custom-call(bf16[32,2048]{1,0:T(8,128)(2,1)} %tokens_h.1, f32[1,2048]{1,0:T(1,128)} %bitcast.4, s32[2,32]{1,0:T(2,128)} %bitcast.6, f32[2,32]{1,0:T(2,128)} %bitcast.7, bf16[1,2048,256]{2,1,0:T(8,128)(2,1)} %w_gate.1, bf16[1,2048,256]{2,1,0:T(8,128)(2,1)} %w_up.1, bf16[1,256,2048]{2,1,0:T(8,128)(2,1)} %w_down.1, ...), custom_call_target="tpu_custom_call" | custom-call | tf_op jit(solution)/shard_map/experts/pallas_call | solution.py:268
  31.0 1.4 %copy.10 = bf16[32,512]{1,0:T(8,128)(2,1)} copy(bf16[32,512]{1,0:T(8,128)(2,1)} %experts.1) | data formatting | bytes 65536
